TPU v7x, 32 devices: a whole 2x2x4 slice. The times are simulated.
32 devices in a mesh: ep: 16 (over z, y, x), tp: 2 (over core).
Axes of the slice: x: 2, y: 2, z: 4, core: 2. Of those that a mesh axis runs over, the one named last changes fastest.
Arguments:
- tokens: bfloat16 [256, 2048], P('ep'), may hold values from -6 to 6
- norm_gain: float32 [2048], replicated, may hold values from 0.1 to 1.9
- query_weight: bfloat16 [2048, 1024], P('ep', 'tp'), may hold values from -0.125 to 0.125
- key_weight: bfloat16 [2048, 1024], P('ep', 'tp'), may hold values from -0.125 to 0.125
- value_weight: bfloat16 [2048, 1024], P('ep', 'tp'), may hold values from -0.125 to 0.125
- outgate_weight: bfloat16 [2048, 1024], P('ep', 'tp'), may hold values from -0.125 to 0.125
- input_weight: bfloat16 [2048, 8], P('ep', 'tp'), may hold values from -0.125 to 0.125
- forget_weight: bfloat16 [2048, 8], P('ep', 'tp'), may hold values from -0.125 to 0.125
- forget_bias: float32 [8], P('tp'), may hold values from -1 to 5
- memory: float32 [256, 8, 128, 128], P('ep', 'tp'), may hold values from -2.4 to 2.4
- stabilizer: float32 [256, 8], P('ep', 'tp'), may hold values from -3 to 3
- head_gain: float32 [1024], P('tp'), may hold values from 0.1 to 1.9
- mix_weight: bfloat16 [1024, 2048], P('tp', 'ep'), may hold values from -0.1875 to 0.1875
- second_gain: float32 [2048], replicated, may hold values from 0.1 to 1.9
- route_experts: int32 [256, 4], P('ep'), may hold values from 0 to 15, all different within a row; in each aligned block of 16 rows (0 to 15, 16 to 31, ...) at most 8 rows name the same one
- route_weight: float32 [256, 4], P('ep'), may hold values from 0.1 to 1
- expert_gate: bfloat16 [16, 2048, 2048], P('ep', None, 'tp'), may hold values from -0.5 to 0.5
- expert_up: bfloat16 [16, 2048, 2048], P('ep', None, 'tp'), may hold values from -0.5 to 0.5
- expert_down: bfloat16 [16, 2048, 2048], P('ep', 'tp'), may hold values from -0.03125 to 0.03125
- dense_gate: bfloat16 [4096, 2048], P(('ep', 'tp')), may hold values from -0.125 to 0.125
- dense_up: bfloat16 [4096, 2048], P(('ep', 'tp')), may hold values from -0.125 to 0.125
- dense_down: bfloat16 [4096, 2048], P(('ep', 'tp')), may hold values from -0.09375 to 0.09375
- branch_scale: float32 [2048], replicated, may hold values from 0.3 to 1.5
Outputs:
- mixed: bfloat16 [256, 2048], P('ep', 'tp')
- memory_new: float32 [256, 8, 128, 128], P('ep', 'tp')
- stabilizer_new: float32 [256, 8], P('ep', 'tp')
Inputs may be any that keep to these rules, and one draw needn't show every extreme that they name: `route_experts`: each row names 4 different experts. Within each aligned block of 16 rows no expert is named by more than 8 rows, and in every draw some expert is named by exactly 8 rows of some block.
All inputs are finite; a program needn't handle non-finite values.
Results may differ from a plain program's by a relative error of at most 0.03.
Values may be sent and summed in bfloat16 or wider, within the bound.
A program may use at most 128 MiB of HBM per device.

v0:
```python
import jax
import jax.numpy as jnp
from jax import lax
from jax.sharding import PartitionSpec as P

norm_eps = 1e-05
clamp_limit = 7.0
sigmoid_slope = 1.702


def rms_scale(values, gain):
    mean_square = jnp.mean(values * values, axis=-1, keepdims=True)
    return values * lax.rsqrt(mean_square + norm_eps) * gain


def round_half(values):
    return lax.optimization_barrier(values.astype(jnp.bfloat16)).astype(jnp.float32)


def clamped_unit(gate_pre, up_pre):
    gate_clamped = jnp.minimum(gate_pre, clamp_limit)
    up_clamped = jnp.clip(up_pre, -clamp_limit, clamp_limit)
    return (
        (up_clamped + 1.0) * gate_clamped * jax.nn.sigmoid(sigmoid_slope * gate_clamped)
    ).astype(jnp.bfloat16)


def memory_step(projected, forget_bias, memory, stabilizer, head_gain):
    query_rows, key_rows, value_rows, outgate_rows, input_pre, forget_pre = projected
    sequences, head_count = stabilizer.shape
    head_size = memory.shape[-1]
    log_forget = jax.nn.log_sigmoid(forget_pre + forget_bias)
    stab_new = jnp.maximum(log_forget + stabilizer, input_pre)
    carried = jnp.exp(log_forget + stabilizer - stab_new)
    written = jnp.exp(input_pre - stab_new)
    query_heads = query_rows.astype(jnp.float32).reshape(sequences, head_count, head_size)
    key_heads = key_rows.astype(jnp.float32).reshape(
        sequences, head_count, head_size
    ) * head_size ** (-0.5)
    value_heads = value_rows.astype(jnp.float32).reshape(sequences, head_count, head_size)
    memory_new = (
        carried[:, :, None, None] * memory
        + written[:, :, None, None] * value_heads[:, :, :, None] * key_heads[:, :, None, :]
    )
    readout = jnp.einsum("bhvk,bhk->bhv", memory_new, query_heads, precision=lax.Precision.HIGHEST)
    out_gate = jax.nn.sigmoid(
        outgate_rows.astype(jnp.float32).reshape(sequences, head_count, head_size)
    )
    gated = (rms_scale(readout, head_gain.reshape(head_count, head_size)) * out_gate).astype(
        jnp.bfloat16
    )
    return (gated.reshape(sequences, head_count * head_size), memory_new, stab_new)


def expert_apply(rows, gate_weight, up_weight, down_weight):
    gate_pre = jnp.dot(rows, gate_weight, preferred_element_type=jnp.float32)
    up_pre = jnp.dot(rows, up_weight, preferred_element_type=jnp.float32)
    activity = clamped_unit(gate_pre, up_pre)
    return jnp.dot(activity, down_weight, preferred_element_type=jnp.float32).astype(jnp.bfloat16)


def slot_table(hit_mask, capacity):
    ranks = jnp.cumsum(hit_mask, axis=1) - 1.0
    slots = jnp.arange(capacity).astype(jnp.float32)
    return hit_mask[:, None, :] * (ranks[:, None, :] == slots[None, :, None]).astype(jnp.float32)


def body(
    tokens,
    norm_gain,
    query_weight,
    key_weight,
    value_weight,
    outgate_weight,
    input_weight,
    forget_weight,
    forget_bias,
    memory,
    stabilizer,
    head_gain,
    mix_weight,
    second_gain,
    route_experts,
    route_weight,
    expert_gate,
    expert_up,
    expert_down,
    dense_gate,
    dense_up,
    dense_down,
    branch_scale,
):
    sequences, model_width = tokens.shape
    ep_count = lax.axis_size("ep")
    tp_count = lax.axis_size("tp")
    part_width = model_width // tp_count
    top_count = route_experts.shape[1]
    expert_count = expert_gate.shape[0] * ep_count
    capacity = max(2, 2 * sequences * top_count // expert_count)
    inputs_float = tokens.astype(jnp.float32)
    normed = rms_scale(inputs_float, norm_gain).astype(jnp.bfloat16)
    weight_list = (
        query_weight,
        key_weight,
        value_weight,
        outgate_weight,
        input_weight,
        forget_weight,
    )
    columns = lax.all_to_all(normed, "ep", split_axis=1, concat_axis=0, tiled=True)
    joined = jnp.concatenate(weight_list, axis=1)
    summed_rows = lax.psum_scatter(
        jnp.dot(columns, joined, preferred_element_type=jnp.float32),
        "ep",
        scatter_dimension=0,
        tiled=True,
    )
    pieces = []
    lower = 0
    for weight in weight_list:
        pieces.append(summed_rows[:, lower : lower + weight.shape[1]])
        lower = lower + weight.shape[1]
    sums = tuple(pieces)
    projected = (
        sums[0].astype(jnp.bfloat16),
        sums[1].astype(jnp.bfloat16),
        sums[2].astype(jnp.bfloat16),
        sums[3].astype(jnp.bfloat16),
        sums[4],
        sums[5],
    )
    gated, memory_new, stab_new = memory_step(projected, forget_bias, memory, stabilizer, head_gain)
    partial_value = jnp.dot(
        gated,
        lax.all_gather(mix_weight, "ep", axis=1, tiled=True),
        preferred_element_type=jnp.float32,
    )
    attended = lax.psum(round_half(partial_value).astype(jnp.bfloat16), "tp").astype(jnp.float32)
    residual = (inputs_float + attended).astype(jnp.bfloat16)
    residual_float = residual.astype(jnp.float32)
    normed_second = rms_scale(residual_float, second_gain).astype(jnp.bfloat16)
    own_residual = lax.dynamic_slice_in_dim(
        residual_float, lax.axis_index("tp") * part_width, part_width, 1
    )
    matched = route_experts[:, :, None] == jnp.arange(expert_count)[None, None, :]
    hit_mask = jnp.any(matched, axis=1).astype(jnp.float32).T
    weights = jnp.sum(jnp.where(matched, route_weight[:, :, None], 0.0), axis=1).T
    select = slot_table(hit_mask, capacity)
    outgoing = jnp.einsum(
        "ecs,sd->ecd",
        select.astype(jnp.bfloat16),
        normed_second,
        preferred_element_type=jnp.float32,
    ).astype(jnp.bfloat16)
    received = lax.all_to_all(outgoing, "ep", split_axis=0, concat_axis=0, tiled=True)
    count = received.shape[1]
    partial_out = expert_apply(
        received.reshape(-1, model_width), expert_gate[0], expert_up[0], expert_down[0]
    )
    halves = lax.psum_scatter(
        partial_out.astype(jnp.float32).astype(jnp.bfloat16), "tp", scatter_dimension=1, tiled=True
    ).astype(jnp.float32)
    returned = lax.all_to_all(
        halves.reshape(ep_count, count, part_width).astype(jnp.bfloat16),
        "ep",
        split_axis=0,
        concat_axis=0,
        tiled=True,
    ).astype(jnp.float32)
    routed = jnp.einsum(
        "ecs,ecd->sd", select * weights[:, None, :], returned, precision=lax.Precision.HIGHEST
    )
    all_rows = lax.all_gather(normed_second, "ep", axis=0, tiled=True)
    gate_rows = jnp.einsum("fd,td->ft", dense_gate, all_rows, preferred_element_type=jnp.float32)
    lift_rows = jnp.einsum("fd,td->ft", dense_up, all_rows, preferred_element_type=jnp.float32)
    activity = (
        (jax.nn.silu(gate_rows) * lift_rows).astype(jnp.bfloat16).reshape(-1, ep_count, sequences)
    )
    down_parts = dense_down.reshape(-1, tp_count, part_width)
    term = jnp.einsum("fjs,fhd->jhsd", activity, down_parts, preferred_element_type=jnp.float32)
    branch = lax.psum_scatter(
        (term * branch_scale.reshape(1, tp_count, 1, part_width)).reshape(-1, part_width),
        ("ep", "tp"),
        scatter_dimension=0,
        tiled=True,
    )
    mixed = own_residual + routed + branch
    return (mixed.astype(jnp.bfloat16), memory_new, stab_new)


def solution(mesh):
    in_specs = (
        P("ep", None),
        P(),
        P("ep", "tp"),
        P("ep", "tp"),
        P("ep", "tp"),
        P("ep", "tp"),
        P("ep", "tp"),
        P("ep", "tp"),
        P("tp"),
        P("ep", "tp", None, None),
        P("ep", "tp"),
        P("tp"),
        P("tp", "ep"),
        P(),
        P("ep", None),
        P("ep", None),
        P("ep", None, "tp"),
        P("ep", None, "tp"),
        P("ep", "tp", None),
        P(("ep", "tp"), None),
        P(("ep", "tp"), None),
        P(("ep", "tp"), None),
        P(),
    )
    out_specs = (P("ep", "tp"), P("ep", "tp", None, None), P("ep", "tp"))
    return jax.shard_map(body, mesh=mesh, in_specs=in_specs, out_specs=out_specs, check_vma=False)
```

profile of v0, /device:TPU:0, one launch (start us, length us, event | category | flops | bytes accessed | tf_op | source)
XLA Modules:
  0.0 416.8 jit_solution(380059310604357217)
XLA Ops:
  8.2 1.6 copy_bitcast_fusion
  9.8 8.3 %all-to-all-start = ((bf16[16,16,128]{2,0,1:T(8,128)(2,1)}), bf16[16,16,128]{2,0,1:T(8,128)(2,1)S(1)}, u32[]{:S(2)}, u32[]{:S(2)}) async-start(bf16[16,16,128]{2,0,1:T(8,128)(2,1)} %copy_bitcast_fusion), calls=%async_computation | async-start | bytes 131072 | tf_op jit(solution)/shard_map/all_to_all | solution.py:110
  21.0 4.7 %all-to-all-done = bf16[16,16,128]{2,0,1:T(8,128)(2,1)S(1)} async-done(((bf16[16,16,128]{2,0,1:T(8,128)(2,1)}), bf16[16,16,128]{2,0,1:T(8,128)(2,1)S(1)}, u32[]{:S(2)}, u32[]{:S(2)}) %all-to-all-start) | async-done | bytes 65568 | tf_op jit(solution)/shard_map/all_to_all | solution.py:110
  25.7 1.8 fusion.72
  28.8 77.2 %reduce-scatter.4.cloned.1.call-done = f32[16,2056]{1,0:T(8,128)} async-done(((f32[256,2056]{1,0:T(8,128)}), f32[16,2056]{1,0:T(8,128)}) %reduce-scatter.4.cloned.1.call-update) | async-done | bytes 131600 | tf_op jit(solution)/shard_map/reduce_scatter | solution.py:112
  108.8 3.0 multiply_add_fusion
  111.8 2.0 copy-done.1
  113.8 3.3 fusion.73
  117.4 51.6 %all-gather.3.cloned.1.call-done = bf16[512,2048]{1,0:T(8,128)(2,1)} async-done(((bf16[512,128]{1,0:T(8,128)(2,1)}), bf16[512,2048]{1,0:T(8,128)(2,1)}) %all-gather.3.cloned.1.call-update) | async-done | bytes 2097168 | tf_op jit(solution)/shard_map/all_gather | solution.py:135
  169.0 2.6 convolution_convert_fusion.1
  171.8 15.9 %all-reduce.2.cloned.1.call-done = bf16[16,2048]{1,0:T(8,128)(2,1)} async-done(((bf16[16,2048]{1,0:T(8,128)(2,1)}), bf16[16,2048]{1,0:T(8,128)(2,1)}) %all-reduce.2.cloned.1.call-update) | async-done | bytes 65552 | tf_op jit(solution)/shard_map/psum | solution.py:138
  190.7 6.8 %all-to-all-start.1 = ((bf16[16,8,2048]{2,1,0:T(8,128)(2,1)}), bf16[16,8,2048]{2,1,0:T(8,128)(2,1)S(1)}, u32[]{:S(2)}, u32[]{:S(2)}) async-start(bf16[16,8,2048]{2,1,0:T(8,128)(2,1)} %convolution_convert_fusion), calls=%async_computation.2 | async-start | bytes 1048576 | tf_op jit(solution)/shard_map/all_to_all | solution.py:155
  198.2 14.9 %all-to-all-done.1 = bf16[16,8,2048]{2,1,0:T(8,128)(2,1)S(1)} async-done(((bf16[16,8,2048]{2,1,0:T(8,128)(2,1)}), bf16[16,8,2048]{2,1,0:T(8,128)(2,1)S(1)}, u32[]{:S(2)}, u32[]{:S(2)}) %all-to-all-start.1) | async-done | bytes 524320 | tf_op jit(solution)/shard_map/all_to_all | solution.py:155
  213.1 2.9 fusion.12
  216.0 5.7 %fusion.6 = bf16[128,2048]{1,0:T(8,128)(2,1)} fusion(bf16[1,1024,2048]{2,1,0:T(8,128)(2,1)} %param.41, f32[128,1024]{1,0:T(8,128)S(1)} %fusion.12, bf16[1,2048,1024]{2,1,0:T(8,128)(2,1)} %param.40, bf16[16,8,2048]{2,1,0:T(8,128)(2,1)S(1)} %all-to-all-done.1), kind=kOutput, calls=%fused_computation.7 | convolution fusion | flops 1075183616 | bytes 9961472 | tf_op jit(solution)/shard_map/dot_general | solution.py:59
  221.9 35.4 %all-gather.5.cloned.1.call-done = bf16[256,2048]{1,0:T(8,128)(2,1)} async-done(((bf16[16,2048]{1,0:T(8,128)(2,1)}), bf16[256,2048]{1,0:T(8,128)(2,1)}) %all-gather.5.cloned.1.call-update) | async-done | bytes 1048592 | tf_op jit(solution)/shard_map/all_gather | solution.py:173
  257.3 1.7 convolution_bitcast_fusion.1
  258.9 1.7 fusion.28
  260.6 1.8 convolution_multiply_fusion
  262.4 3.8 reduce-scatter.6.cloned.1.call-done
  266.2 6.7 %all-to-all-start.2 = ((bf16[16,8,1024]{2,1,0:T(8,128)(2,1)}), bf16[16,8,1024]{2,1,0:T(8,128)(2,1)S(1)}, u32[]{:S(2)}, u32[]{:S(2)}) async-start(bf16[16,8,1024]{2,1,0:T(8,128)(2,1)} %bitcast.100), calls=%async_computation.4 | async-start | bytes 524288 | tf_op jit(solution)/shard_map/all_to_all | solution.py:163
  273.6 10.3 %all-to-all-done.2 = bf16[16,8,1024]{2,1,0:T(8,128)(2,1)S(1)} async-done(((bf16[16,8,1024]{2,1,0:T(8,128)(2,1)}), bf16[16,8,1024]{2,1,0:T(8,128)(2,1)S(1)}, u32[]{:S(2)}, u32[]{:S(2)}) %all-to-all-start.2) | async-done | bytes 262176 | tf_op jit(solution)/shard_map/all_to_all | solution.py:163
  284.0 124.0 %reduce-scatter.8.cloned.1.call-done = f32[16,1024]{1,0:T(8,128)} async-done(((f32[512,1024]{1,0:T(8,128)}), f32[16,1024]{1,0:T(8,128)}) %reduce-scatter.8.cloned.1.call-update) | async-done | bytes 65552 | tf_op jit(solution)/shard_map/reduce_scatter | solution.py:181
  407.9 2.0 fusion.31
  (72 shorter events, 12.7 us)
Async XLA Ops:
  7.2 250.1 %copy-start = (bf16[128,2048]{1,0:T(8,128)(2,1)S(1)}, bf16[128,2048]{1,0:T(8,128)(2,1)}, u32[]{:S(2)}) copy-start(bf16[128,2048]{1,0:T(8,128)(2,1)} %param.42) | copy-start | bytes 1572868
  7.2 21.1 %copy-start.8 = (f32[16,4]{0,1:T(4,128)S(1)}, f32[16,4]{0,1:T(4,128)}, u32[]{:S(2)}) copy-start(f32[16,4]{0,1:T(4,128)} %param.33) | copy-start | bytes 772
  7.2 21.2 %copy-start.7 = (s32[16,4]{0,1:T(4,128)S(1)}, s32[16,4]{0,1:T(4,128)}, u32[]{:S(2)}) copy-start(s32[16,4]{0,1:T(4,128)} %param.37) | copy-start | bytes 772
  7.2 99.9 %copy-start.11 = (f32[4]{0:T(128)S(1)}, f32[4]{0:T(128)}, u32[]{:S(2)}) copy-start(f32[4]{0:T(128)} %param.31) | copy-start | bytes 52
  9.8 15.9 %all-to-all-start = ((bf16[16,16,128]{2,0,1:T(8,128)(2,1)}), bf16[16,16,128]{2,0,1:T(8,128)(2,1)S(1)}, u32[]{:S(2)}, u32[]{:S(2)}) async-start(bf16[16,16,128]{2,0,1:T(8,128)(2,1)} %copy_bitcast_fusion), calls=%async_computation | async-start | bytes 131072 | tf_op jit(solution)/shard_map/all_to_all | solution.py:110
  18.2 87.9 %reduce-scatter.4.cloned.1.call-start = ((), (), s32[]{:S(2)}) async-start(), calls=%async_computation.6 | async-start | bytes 2367488 | tf_op jit(solution)/shard_map/reduce_scatter | solution.py:112
  27.5 141.5 %all-gather.3.cloned.1.call-start = ((), (), s32[]{:S(2)}) async-start(), calls=%async_computation.7 | async-start | bytes 2228224 | tf_op jit(solution)/shard_map/all_gather | solution.py:135
  28.3 159.5 %all-reduce.2.cloned.1.call-start = ((), (), s32[]{:S(2)}) async-start(), calls=%async_computation.8 | async-start | bytes 131072 | tf_op jit(solution)/shard_map/psum | solution.py:138
  111.8 2.0 copy-start.1
  113.8 3.5 copy-start.9
  113.8 73.9 %copy-start.2 = (bf16[16,2048]{1,0:T(8,128)(2,1)S(1)}, bf16[16,2048]{1,0:T(8,128)(2,1)}, u32[]{:S(2)}) copy-start(bf16[16,2048]{1,0:T(8,128)(2,1)} %param.23) | copy-start | bytes 196612
  113.8 74.9 %copy-start.5 = (f32[2048]{0:T(1024)S(1)}, f32[2048]{0:T(1024)}, u32[]{:S(2)}) copy-start(f32[2048]{0:T(1024)} %param.36) | copy-start | bytes 24580
  189.6 8.0 %copy-start.3 = (bf16[16,2048]{1,0:T(8,128)(2,1)}, bf16[16,2048]{1,0:T(8,128)(2,1)S(1)}, u32[]{:S(2)}) copy-start(bf16[16,2048]{1,0:T(8,128)(2,1)S(1)} %multiply_convert_fusion) | copy-start | bytes 196612
  190.7 22.3 %all-to-all-start.1 = ((bf16[16,8,2048]{2,1,0:T(8,128)(2,1)}), bf16[16,8,2048]{2,1,0:T(8,128)(2,1)S(1)}, u32[]{:S(2)}, u32[]{:S(2)}) async-start(bf16[16,8,2048]{2,1,0:T(8,128)(2,1)} %convolution_convert_fusion), calls=%async_computation.2 | async-start | bytes 1048576 | tf_op jit(solution)/shard_map/all_to_all | solution.py:155
  197.6 59.7 %all-gather.5.cloned.1.call-start = ((), (), s32[]{:S(2)}) async-start(), calls=%async_computation.10 | async-start | bytes 1114112 | tf_op jit(solution)/shard_map/all_gather | solution.py:173
  198.2 68.0 %reduce-scatter.6.cloned.1.call-start = ((), (), s32[]{:S(2)}) async-start(), calls=%async_computation.9 | async-start | bytes 786432 | tf_op jit(solution)/shard_map/reduce_scatter | solution.py:160
  216.0 5.8 %copy-start.6 = (f32[2048]{0:T(1024)S(1)}, f32[2048]{0:T(1024)}, u32[]{:S(2)}) copy-start(f32[2048]{0:T(1024)} %param.45) | copy-start | bytes 24580
  216.0 43.0 %copy-start.12 = (bf16[128,2048]{1,0:T(8,128)(2,1)S(1)}, bf16[128,2048]{1,0:T(8,128)(2,1)}, u32[]{:S(2)}) copy-start(bf16[128,2048]{1,0:T(8,128)(2,1)} %param.43) | copy-start | bytes 1572868
  221.7 38.9 %copy-start.4 = (bf16[128,2048]{1,0:T(8,128)(2,1)S(1)}, bf16[128,2048]{1,0:T(8,128)(2,1)}, u32[]{:S(2)}) copy-start(bf16[128,2048]{1,0:T(8,128)(2,1)} %param.44) | copy-start | bytes 1572868
  221.8 186.2 %reduce-scatter.8.cloned.1.call-start = ((), (), s32[]{:S(2)}) async-start(), calls=%async_computation.11 | async-start | bytes 2162688 | tf_op jit(solution)/shard_map/reduce_scatter | solution.py:181
  221.8 51.1 %copy-start.10 = (f32[16,4]{0,1:T(4,128)S(1)}, f32[16,4]{0,1:T(4,128)}, u32[]{:S(2)}) copy-start(f32[16,4]{0,1:T(4,128)} %param.38) | copy-start | bytes 772
  266.2 17.8 %all-to-all-start.2 = ((bf16[16,8,1024]{2,1,0:T(8,128)(2,1)}), bf16[16,8,1024]{2,1,0:T(8,128)(2,1)S(1)}, u32[]{:S(2)}, u32[]{:S(2)}) async-start(bf16[16,8,1024]{2,1,0:T(8,128)(2,1)} %bitcast.100), calls=%async_computation.4 | async-start | bytes 524288 | tf_op jit(solution)/shard_map/all_to_all | solution.py:163
Sparse Core Ops, SparseCore 0:
  27.6 78.3 reduce-scatter.3
  108.7 60.2 all-gather.2
  171.8 15.9 all-reduce.1
  200.8 56.3 all-gather.4
  259.4 6.7 reduce-scatter.5
  268.3 139.6 reduce-scatter.7
where the time goes:
time: 418 us; the launch traced here: 417 us
  waiting for transfers between devices  339 us (81%)
  matrix products  24.5 us (6%)
  starting transfers between devices  22.1 us (5%)
  between operations  14.4 us (3%)
  other arithmetic  10.8 us (3%)
  local copies, waits for them, and re-layouts  5.91 us (1%)
    reduce_scatter x1, waiting for transfers between devices, body(): lax.psum_scatter((term * branch_scale.reshape(1, tp_count, 1, part_width)...  124 us
    reduce_scatter x1, waiting for transfers between devices, body(): lax.psum_scatter(jnp.dot(columns, joined, preferred_element_type=jnp.floa...  77.2 us
    all_gather x1, waiting for transfers between devices, body(): lax.all_gather(mix_weight, 'ep', axis=1, tiled=True)  51.6 us
    all_gather x1, waiting for transfers between devices, body(): all_rows = lax.all_gather(normed_second, 'ep', axis=0, tiled=True)  35.4 us
    psum x1, waiting for transfers between devices, body(): lax.psum(round_half(partial_value).astype(jnp.bfloat16), 'tp')  15.9 us
    all_to_all x1, waiting for transfers between devices, body(): lax.all_to_all(outgoing, 'ep', split_axis=0, concat_axis=0, tiled=True)  14.9 us
    all_to_all x1, waiting for transfers between devices, body(): lax.all_to_all(halves.reshape(ep_count, count, part_width).astype(jnp.bfl...  10.3 us
  transfers between devices with their start and end apart: 9, of which 9 were waited for; matrix products, arithmetic and copies ran while one was open for 7% of the time, Pallas kernels for 0%

commit v1 on v0

v1 whole, which is shorter than its diff:
```python
import functools

import jax
import jax.numpy as jnp
from jax import lax
from jax.experimental import pallas as pl
from jax.experimental.pallas import tpu as pltpu
from jax.sharding import PartitionSpec as P

norm_eps = 1e-05
clamp_limit = 7.0
sigmoid_slope = 1.702


def rms_scale(values, gain):
    mean_square = jnp.mean(values * values, axis=-1, keepdims=True)
    return values * lax.rsqrt(mean_square + norm_eps) * gain


def clamped_unit(gate_pre, up_pre):
    gate_clamped = jnp.minimum(gate_pre, clamp_limit)
    up_clamped = jnp.clip(up_pre, -clamp_limit, clamp_limit)
    return (
        (up_clamped + 1.0) * gate_clamped * jax.nn.sigmoid(sigmoid_slope * gate_clamped)
    ).astype(jnp.bfloat16)


def memory_step(projected, forget_bias, memory, stabilizer, head_gain):
    query_rows, key_rows, value_rows, outgate_rows, input_pre, forget_pre = projected
    sequences, head_count = stabilizer.shape
    head_size = memory.shape[-1]
    log_forget = jax.nn.log_sigmoid(forget_pre + forget_bias)
    stab_new = jnp.maximum(log_forget + stabilizer, input_pre)
    carried = jnp.exp(log_forget + stabilizer - stab_new)
    written = jnp.exp(input_pre - stab_new)
    query_heads = query_rows.astype(jnp.float32).reshape(sequences, head_count, head_size)
    key_heads = key_rows.astype(jnp.float32).reshape(
        sequences, head_count, head_size
    ) * head_size ** (-0.5)
    value_heads = value_rows.astype(jnp.float32).reshape(sequences, head_count, head_size)
    memory_new = (
        carried[:, :, None, None] * memory
        + written[:, :, None, None] * value_heads[:, :, :, None] * key_heads[:, :, None, :]
    )
    readout = jnp.einsum("bhvk,bhk->bhv", memory_new, query_heads, precision=lax.Precision.HIGHEST)
    out_gate = jax.nn.sigmoid(
        outgate_rows.astype(jnp.float32).reshape(sequences, head_count, head_size)
    )
    gated = (rms_scale(readout, head_gain.reshape(head_count, head_size)) * out_gate).astype(
        jnp.bfloat16
    )
    return (gated.reshape(sequences, head_count * head_size), memory_new, stab_new)


def meet(count, me):
    barrier = pltpu.get_barrier_semaphore()

    def greet(step, carry):
        pl.semaphore_signal(
            barrier,
            inc=1,
            device_id={"ep": lax.rem(me + step, count)},
            device_id_type=pl.DeviceIdType.MESH,
        )
        return carry

    lax.fori_loop(1, count, greet, 0)
    pl.semaphore_wait(barrier, count - 1)


def link(count, me, step, source, landing, send_sem, recv_sem, gather):
    peer = lax.rem(me + step, count)
    return pltpu.make_async_remote_copy(
        src_ref=source if gather else source.at[peer],
        dst_ref=landing.at[me],
        send_sem=send_sem.at[step],
        recv_sem=recv_sem.at[step],
        device_id={"ep": peer},
        device_id_type=pl.DeviceIdType.MESH,
    )


def exchange_kernel(count, gather, source, landing, send_sem, recv_sem):
    me = lax.axis_index("ep")
    meet(count, me)

    def start(step, carry):
        link(count, me, step, source, landing, send_sem, recv_sem, gather).start()
        return carry

    def finish(step, carry):
        link(count, me, step, source, landing, send_sem, recv_sem, gather).wait()
        return carry

    lax.fori_loop(1, count, start, 0)
    landing[me] = source[...] if gather else source[me]
    lax.fori_loop(1, count, finish, 0)


def sum_kernel(count, source, total, landing, send_sem, recv_sem):
    me = lax.axis_index("ep")
    meet(count, me)

    def start(step, carry):
        link(count, me, step, source, landing, send_sem, recv_sem, False).start()
        return carry

    def finish(step, carry):
        link(count, me, step, source, landing, send_sem, recv_sem, False).wait()
        total[...] += landing[lax.rem(me + count - step, count)].astype(jnp.float32)
        return carry

    lax.fori_loop(1, count, start, 0)
    total[...] = source[me].astype(jnp.float32)
    lax.fori_loop(1, count, finish, 0)


def semaphores(count):
    return [pltpu.SemaphoreType.DMA((count,)), pltpu.SemaphoreType.DMA((count,))]


def in_vmem():
    return pl.BlockSpec(memory_space=pltpu.VMEM)


def exchange(blocks, count, name, gather=False):
    shape = (count,) + blocks.shape if gather else blocks.shape
    return pl.pallas_call(
        functools.partial(exchange_kernel, count, gather),
        out_shape=jax.ShapeDtypeStruct(shape, blocks.dtype),
        in_specs=[in_vmem()],
        out_specs=in_vmem(),
        scratch_shapes=semaphores(count),
        compiler_params=pltpu.CompilerParams(
            collective_id=name, has_side_effects=True, vmem_limit_bytes=16 * 2**20
        ),
    )(blocks)


def exchange_sum(blocks, count, name):
    return pl.pallas_call(
        functools.partial(sum_kernel, count),
        out_shape=jax.ShapeDtypeStruct(blocks.shape[1:], jnp.float32),
        in_specs=[in_vmem()],
        out_specs=in_vmem(),
        scratch_shapes=[pltpu.VMEM(blocks.shape, blocks.dtype)] + semaphores(count),
        compiler_params=pltpu.CompilerParams(
            collective_id=name, has_side_effects=True, vmem_limit_bytes=24 * 2**20
        ),
    )(blocks)


def split_parts(values, number):
    parts = []
    for _ in range(number):
        part = lax.reduce_precision(values, 8, 7)
        parts.append(part.astype(jnp.bfloat16))
        values = values - part
    return parts


def body(
    tokens,
    norm_gain,
    query_weight,
    key_weight,
    value_weight,
    outgate_weight,
    input_weight,
    forget_weight,
    forget_bias,
    memory,
    stabilizer,
    head_gain,
    mix_weight,
    second_gain,
    route_experts,
    route_weight,
    expert_gate,
    expert_up,
    expert_down,
    dense_gate,
    dense_up,
    dense_down,
    branch_scale,
):
    sequences, model_width = tokens.shape
    ep_count = lax.axis_size("ep")
    tp_count = lax.axis_size("tp")
    me, side = lax.axis_index("ep"), lax.axis_index("tp")
    swap = [(i, tp_count - 1 - i) for i in range(tp_count)]
    rows = sequences * ep_count
    part_width = model_width // tp_count
    own_width = model_width // ep_count
    lanes = 128
    first = side == 0

    inputs_float = tokens.astype(jnp.float32)
    normed = rms_scale(inputs_float, norm_gain).astype(jnp.bfloat16)
    matched = route_experts[:, :, None] == jnp.arange(ep_count)[None, None, :]
    weights = jnp.sum(jnp.where(matched, route_weight[:, :, None], 0.0), axis=1)
    weight_parts = jnp.stack(split_parts(weights, 3), axis=-1)
    weight_parts = jnp.pad(weight_parts, ((0, 0), (0, 0), (0, lanes - 3)))
    payload = jnp.concatenate(
        [
            normed.reshape(sequences, ep_count, own_width),
            tokens.reshape(sequences, ep_count, own_width),
            weight_parts,
        ],
        axis=2,
    ).transpose(1, 0, 2)
    columns = exchange(payload, ep_count, 1).reshape(rows, -1)
    token_columns = columns[:, own_width : 2 * own_width]
    row_weight = jnp.sum(
        columns[:, 2 * own_width : 2 * own_width + 3].astype(jnp.float32), axis=1, keepdims=True
    )

    wide = jnp.concatenate((query_weight, key_weight, value_weight, outgate_weight), axis=1)
    thin = jnp.concatenate((input_weight, forget_weight), axis=1)
    own_columns = columns[:, :own_width]
    wide_sums = jnp.dot(own_columns, wide, preferred_element_type=jnp.float32)
    thin_sums = jnp.dot(own_columns, thin, preferred_element_type=jnp.float32)
    gates = thin.shape[1]
    upper, under = split_parts(thin_sums, 2)
    partials = jnp.concatenate(
        [
            wide_sums.astype(jnp.bfloat16),
            jnp.pad(jnp.concatenate([upper, under], axis=1), ((0, 0), (0, lanes - 2 * gates))),
        ],
        axis=1,
    )
    sums = exchange_sum(partials.reshape(ep_count, sequences, -1), ep_count, 2)
    width = query_weight.shape[1]
    gate_sums = sums[:, 4 * width : 4 * width + gates] + sums[:, 4 * width + gates : 4 * width + 2 * gates]
    projected = tuple(
        sums[:, i * width : (i + 1) * width].astype(jnp.bfloat16) for i in range(4)
    ) + (gate_sums[:, : gates // 2], gate_sums[:, gates // 2 :])
    gated, memory_new, stab_new = memory_step(projected, forget_bias, memory, stabilizer, head_gain)

    all_gated = exchange(gated, ep_count, 3, gather=True).reshape(rows, -1)
    partial_value = jnp.dot(
        all_gated, mix_weight, preferred_element_type=jnp.float32
    ).astype(jnp.bfloat16)
    half = rows // tp_count
    upper, under = partial_value[:half], partial_value[half:]
    kept = jnp.where(first, upper, under)
    came = lax.ppermute(jnp.where(first, under, upper), "tp", swap)
    attended = kept.astype(jnp.float32) + came.astype(jnp.float32)
    token_half = jnp.where(first, token_columns[:half], token_columns[half:])
    residual_part = (token_half.astype(jnp.float32) + attended).astype(jnp.bfloat16)
    half_rows = exchange(residual_part, ep_count, 4, gather=True)
    half_rows = half_rows.transpose(1, 0, 2).reshape(half, model_width)
    other_rows = lax.ppermute(half_rows, "tp", swap)
    residual = jnp.concatenate(
        [jnp.where(first, half_rows, other_rows), jnp.where(first, other_rows, half_rows)], axis=0
    )
    normed_second = rms_scale(residual.astype(jnp.float32), second_gain).astype(jnp.bfloat16)

    gate_pre = jnp.dot(normed_second, expert_gate[0], preferred_element_type=jnp.float32)
    up_pre = jnp.dot(normed_second, expert_up[0], preferred_element_type=jnp.float32)
    expert_act = clamped_unit(gate_pre, up_pre)
    expert_out = jnp.dot(expert_act, expert_down[0], preferred_element_type=jnp.float32)
    gate_rows = jnp.einsum(
        "td,fd->tf", normed_second, dense_gate, preferred_element_type=jnp.float32
    )
    lift_rows = jnp.einsum("td,fd->tf", normed_second, dense_up, preferred_element_type=jnp.float32)
    dense_act = (jax.nn.silu(gate_rows) * lift_rows).astype(jnp.bfloat16)
    dense_out = jnp.dot(dense_act, dense_down, preferred_element_type=jnp.float32)
    term = dense_out * branch_scale + row_weight * expert_out
    left, right = term[:, :part_width], term[:, part_width:]
    passed = jnp.where(first, right, left).astype(jnp.bfloat16)
    received = lax.ppermute(passed, "tp", swap).astype(jnp.float32)
    summed = (jnp.where(first, left, right) + received).astype(jnp.bfloat16)
    branches = exchange_sum(summed.reshape(ep_count, sequences, part_width), ep_count, 5)
    own_residual = lax.dynamic_slice(
        residual, (me * sequences, side * part_width), (sequences, part_width)
    )
    mixed = own_residual.astype(jnp.float32) + branches
    return (mixed.astype(jnp.bfloat16), memory_new, stab_new)


def solution(mesh):
    in_specs = (
        P("ep", None),
        P(),
        P("ep", "tp"),
        P("ep", "tp"),
        P("ep", "tp"),
        P("ep", "tp"),
        P("ep", "tp"),
        P("ep", "tp"),
        P("tp"),
        P("ep", "tp", None, None),
        P("ep", "tp"),
        P("tp"),
        P("tp", "ep"),
        P(),
        P("ep", None),
        P("ep", None),
        P("ep", None, "tp"),
        P("ep", None, "tp"),
        P("ep", "tp", None),
        P(("ep", "tp"), None),
        P(("ep", "tp"), None),
        P(("ep", "tp"), None),
        P(),
    )
    out_specs = (P("ep", "tp"), P("ep", "tp", None, None), P("ep", "tp"))
    return jax.shard_map(body, mesh=mesh, in_specs=in_specs, out_specs=out_specs, check_vma=False)
```

time: 418 us -> 119 us (0.28)
  waiting for transfers between devices: 339 us -> 4.44 us
  Pallas kernels: 0 us -> 80.4 us
  starting transfers between devices: 22.1 us -> 0.28 us
  between operations: 14.4 us -> 1.06 us
  matrix products: 24.5 us -> 19.7 us
  local copies, waits for them, and re-layouts: 5.91 us -> 1.28 us
    reduce_scatter x3 -> x0, waiting for transfers between devices: 205 us -> none  [the longest x1 124 us: body(): lax.psum_scatter((term * branch_scale.reshape(1, tp_count, 1, part_width)...]
    all_gather x2 -> x0, waiting for transfers between devices: 87 us -> none  [the longest x1 51.6 us: body(): lax.all_gather(mix_weight, 'ep', axis=1, tiled=True)]
    pallas_call x0 -> x5, Pallas kernels: none -> 80.4 us  [the longest x3 40.5 us: exchange(): pl.pallas_call(functools.partial(exchange_kernel, count, gather), out_sha...]
    all_to_all x3 -> x0, waiting for transfers between devices: 29.9 us -> none  [the longest x1 14.9 us: body(): lax.all_to_all(outgoing, 'ep', split_axis=0, concat_axis=0, tiled=True)]
    all_to_all x3 -> x0, starting transfers between devices: 21.9 us -> none  [the longest x1 8.34 us: body(): lax.all_to_all(normed, 'ep', split_axis=1, concat_axis=0, tiled=True)]
    psum x1 -> x0, waiting for transfers between devices: 15.9 us -> none  [body(): lax.psum(round_half(partial_value).astype(jnp.bfloat16), 'tp')]
    dot_general x9 -> x7, matrix products: 21.2 us -> 16.3 us  [the longest x1 7.68 us: body(): jnp.dot(expert_act, expert_down[0], preferred_element_type=jnp.float32)]
    ppermute x0 -> x3, waiting for transfers between devices: none -> 4.44 us  [the longest x1 1.79 us: body(): other_rows = lax.ppermute(half_rows, 'tp', swap)]
  transfers between devices with their start and end apart: 9 -> 3, of which waited for: 9 -> 3; matrix products, arithmetic and copies ran while one was open for 7% -> 1% of each run, Pallas kernels for 0% -> 0%
where the time goes in v1:
time: 119 us; the launch traced here: 117 us
  Pallas kernels  80.4 us (68%)
  matrix products  19.7 us (17%)
  other arithmetic  9.97 us (8%)
  waiting for transfers between devices  4.44 us (4%)
  local copies, waits for them, and re-layouts  1.28 us (1%)
    pallas_call x3, Pallas kernels, exchange(): pl.pallas_call(functools.partial(exchange_kernel, count, gather), out_sha...  40.5 us
    pallas_call x2, Pallas kernels, exchange_sum(): pl.pallas_call(functools.partial(sum_kernel, count), out_shape=jax.ShapeD...  39.9 us
    dot_general x1, matrix products, body(): jnp.dot(expert_act, expert_down[0], preferred_element_type=jnp.float32)  7.68 us
    dot_general x1, matrix products, memory_step(): jnp.einsum('bhvk,bhk->bhv', memory_new, query_heads, precision=lax.Precis...  3.35 us
    dot_general x1, matrix products, body(): jnp.dot(dense_act, dense_down, preferred_element_type=jnp.float32)  3.25 us
    add x1, other arithmetic, memory_step(): carried[:, :, None, None] * memory  3.04 us
  transfers between devices with their start and end apart: 3, of which 3 were waited for; matrix products, arithmetic and copies ran while one was open for 1% of the time, Pallas kernels for 0%

profile of v1, /device:TPU:0, one launch (start us, length us, event | category | flops | bytes accessed | tf_op | source)
XLA Modules:
  0.0 117.1 jit_solution(17201675163299540545)
XLA Ops:
  0.6 0.8 select_reduce_fusion
  1.7 1.0 fusion.49
  2.7 1.0 copy_bitcast_fusion.1
  3.7 10.7 %shard_map.238 = bf16[16,16,384]{2,1,0:T(8,128)(2,1)S(1)} custom-call(bf16[16,16,384]{2,1,0:T(8,128)(2,1)S(1)} %fusion.48.source), custom_call_target="tpu_custom_call" | custom-call | tf_op jit(solution)/shard_map/pallas_call | solution.py:128
  14.4 0.8 reduce-precision_convert_fusion
  15.4 1.5 %convolution_convert_fusion = bf16[256,2048]{1,0:T(8,128)(2,1)S(1)} fusion(bf16[128,512]{1,0:T(8,128)(2,1)} %param.28, bf16[128,512]{1,0:T(8,128)(2,1)} %param.27, bf16[128,512]{1,0:T(8,128)(2,1)} %param.26, bf16[128,512]{1,0:T(8,128)(2,1)} %param.25, bf16[256,384]{1,0:T(8,128)(2,1)S(1)} %bitcast.78), kind=kOutput, calls=%fused_computation.12 | convolution fusion | flops 136839168 | bytes 1638400 | tf_op jit(solution)/shard_map/dot_general | solution.py:221
  17.0 22.9 %shard_map.239 = f32[16,2176]{1,0:T(8,128)S(1)} custom-call(bf16[16,16,2176]{2,1,0:T(8,128)(2,1)S(1)} %bitcast.74), custom_call_target="tpu_custom_call" | custom-call | tf_op jit(solution)/shard_map/pallas_call | solution.py:141
  40.4 3.0 %multiply_add_fusion = f32[16,4,128,128]{3,2,1,0:T(8,128)S(1)} fusion(f32[16,4,128,128]{3,2,1,0:T(8,128)} %param.32, f32[16,4,128]{2,1,0:T(4,128)S(1)} %mul.162, f32[16,4,128]{2,1,0:T(4,128)S(1)} %broadcast_multiply_fusion, f32[16,4]{1,0:T(8,128)S(1)} %get-tuple-element.15), kind=kLoop, calls=%fused_computation.6 | loop fusion | flops 3145728 | bytes 8454400 | tf_op jit(solution)/shard_map/add | solution.py:42
  43.5 3.3 %fusion.85 = f32[16,4,1,128]{3,2,1,0:T(1,128)S(1)} fusion(f32[16,4,128,128]{3,2,1,0:T(8,128)S(1)} %multiply_add_fusion, bf16[16,4,128,1]{2,3,1,0:T(2,128)(2,1)S(1)} %reshape.141), kind=kOutput, calls=%fused_computation.114 | convolution fusion | flops 12582912 | bytes 4243456 | tf_op jit(solution)/shard_map/bhvk,bhk->bhv/dot_general | solution.py:45
  47.1 15.1 %shard_map.240 = bf16[16,16,512]{2,1,0:T(8,128)(2,1)S(1)} custom-call(bf16[16,512]{1,0:T(8,128)(2,1)S(1)} %bitcast.81), custom_call_target="tpu_custom_call" | custom-call | tf_op jit(solution)/shard_map/pallas_call | solution.py:128
  62.5 1.2 %collective-permute-done = bf16[128,128]{1,0:T(8,128)(2,1)S(1)} collective-permute-done((bf16[128,128]{1,0:T(8,128)(2,1)S(1)}, bf16[128,128]{1,0:T(8,128)(2,1)S(1)}, u32[]{:S(2)}, u32[]{:S(2)}) %collective-permute-start) | collective-permute-done | bytes 32800 | tf_op jit(solution)/shard_map/ppermute | solution.py:247
  63.8 14.7 %shard_map.241 = bf16[16,128,128]{2,1,0:T(8,128)(2,1)S(1)} custom-call(bf16[128,128]{1,0:T(8,128)(2,1)S(1)} %add_convert_fusion.2.source), custom_call_target="tpu_custom_call" | custom-call | tf_op jit(solution)/shard_map/pallas_call | solution.py:128
  78.8 1.8 %collective-permute-done.1 = bf16[128,2048]{1,0:T(8,128)(2,1)S(1)} collective-permute-done((bf16[128,2048]{1,0:T(8,128)(2,1)S(1)}, bf16[128,2048]{1,0:T(8,128)(2,1)S(1)}, u32[]{:S(2)}, u32[]{:S(2)}) %collective-permute-start.1) | collective-permute-done | bytes 524320 | tf_op jit(solution)/shard_map/ppermute | solution.py:253
  80.8 0.3 fusion.11
  81.1 2.3 %fusion.14 = f32[256,1024]{1,0:T(8,128)} fusion(bf16[1,2048,1024]{2,1,0:T(8,128)(2,1)S(1)} %copy-done.10, f32[2048]{0:T(1024)S(1)} %copy-done.5, f32[256]{0:T(256)S(1)} %add_rsqrt_fusion.1, bf16[128,2048]{1,0:T(8,128)(2,1)S(1)} %get-tuple-element.18, bf16[128,2048]{1,0:T(8,128)(2,1)S(1)} %get-tuple-element.17), kind=kOutput, calls=%fused_computation.18 | convolution fusion | flops 1077673984 | bytes 6300672 | tf_op jit(solution)/shard_map/dot_general | solution.py:259
  83.4 0.5 fusion.82
  84.0 7.7 %fusion.6 = f32[256,2048]{1,0:T(8,128)} fusion(bf16[1,1024,2048]{2,1,0:T(8,128)(2,1)} %param.41, f32[256]{0:T(256)S(1)} %convert_reduce_fusion, f32[256,1024]{1,0:T(8,128)} %fusion.14, bf16[1,2048,1024]{2,1,0:T(8,128)(2,1)} %param.40, f32[2048]{0:T(1024)S(1)} %copy-done.5, f32[256]{0:T(256)S(1)} %add_rsqrt_fusion.1, ...), kind=kOutput, calls=%fused_computation.7 | convolution fusion | flops 2154037248 | bytes 12593152 | tf_op jit(solution)/shard_map/dot_general | solution.py:262
  91.6 3.2 %fusion.9 = f32[256,2048]{1,0:T(8,128)S(1)} fusion(f32[256,2048]{1,0:T(8,128)} %fusion.6, bf16[128,2048]{1,0:T(8,128)(2,1)S(1)} %copy-done, f32[2048]{0:T(1024)S(1)} %copy-done.6, f32[256,128]{1,0:T(8,128)S(1)} %fusion.82, bf16[128,2048]{1,0:T(8,128)(2,1)} %param.43, f32[2048]{0:T(1024)S(1)} %copy-done.5, f32[256]{0:T(256)S(1)} %add_rsqrt_fusion.1, ...), kind=kOutput, calls=%fused_computation.9 | convolution fusion | flops 273350656 | bytes 6439936 | tf_op jit(solution)/shard_map/dot_general | solution.py:268
  94.9 0.9 select_convert_fusion
  95.9 0.7 copy.59
  96.6 1.5 %collective-permute-done.2 = bf16[256,1024]{1,0:T(8,128)(2,1)} collective-permute-done((bf16[256,1024]{1,0:T(8,128)(2,1)}, bf16[256,1024]{1,0:T(8,128)(2,1)}, u32[]{:S(2)}, u32[]{:S(2)}) %collective-permute-start.2) | collective-permute-done | bytes 524320 | tf_op jit(solution)/shard_map/ppermute | solution.py:272
  98.0 1.3 %add_convert_fusion = bf16[256,1024]{1,0:T(8,128)(2,1)S(1)} fusion(bf16[256,1024]{1,0:T(8,128)(2,1)} %collective-permute-done.2, f32[256,2048]{1,0:T(8,128)S(1)} %fusion.9, pred[]{:T(512)S(6)} %eq.16), kind=kLoop, calls=%fused_computation.29 | loop fusion | flops 1048576 | bytes 3145729 | tf_op jit(solution)/shard_map/convert_element_type | solution.py:273
  99.4 17.0 %shard_map.242 = f32[16,1024]{1,0:T(8,128)S(1)} custom-call(bf16[16,16,1024]{2,1,0:T(8,128)(2,1)S(1)} %bitcast.75), custom_call_target="tpu_custom_call" | custom-call | tf_op jit(solution)/shard_map/pallas_call | solution.py:141
  116.4 0.7 add_convert_fusion.1
  (58 shorter events, 2.1 us)
Async XLA Ops:
  0.6 91.0 %copy-start = (bf16[128,2048]{1,0:T(8,128)(2,1)S(1)}, bf16[128,2048]{1,0:T(8,128)(2,1)}, u32[]{:S(2)}) copy-start(bf16[128,2048]{1,0:T(8,128)(2,1)} %param.44) | copy-start | bytes 1572868
  16.9 23.2 %copy-start.7 = (f32[16,4]{0,1:T(4,128)S(1)}, f32[16,4]{0,1:T(4,128)}, u32[]{:S(2)}) copy-start(f32[16,4]{0,1:T(4,128)} %param.33) | copy-start | bytes 772
  16.9 23.3 %copy-start.9 = (f32[4]{0:T(128)S(1)}, f32[4]{0:T(128)}, u32[]{:S(2)}) copy-start(f32[4]{0:T(128)} %param.31) | copy-start | bytes 52
  43.5 3.4 %copy-start.1 = (f32[16,4,128,128]{3,2,1,0:T(8,128)}, f32[16,4,128,128]{3,2,1,0:T(8,128)S(1)}, u32[]{:S(2)}) copy-start(f32[16,4,128,128]{3,2,1,0:T(8,128)S(1)} %multiply_add_fusion) | copy-start | bytes 12582916
  43.5 3.5 %copy-start.8 = (f32[512]{0:T(512)S(1)}, f32[512]{0:T(512)}, u32[]{:S(2)}) copy-start(f32[512]{0:T(512)} %param.34) | copy-start | bytes 6148
  43.5 18.7 %copy-start.4 = (bf16[512,128]{1,0:T(8,128)(2,1)S(1)}, bf16[512,128]{1,0:T(8,128)(2,1)}, u32[]{:S(2)}) copy-start(bf16[512,128]{1,0:T(8,128)(2,1)} %param.35) | copy-start | bytes 393220
  62.5 1.3 %collective-permute-start = (bf16[128,128]{1,0:T(8,128)(2,1)S(1)}, bf16[128,128]{1,0:T(8,128)(2,1)S(1)}, u32[]{:S(2)}, u32[]{:S(2)}) collective-permute-start(bf16[128,128]{1,0:T(8,128)(2,1)S(1)} %broadcast_select_fusion.2), channel_id=1, source_target_pairs={{0,1},{1,0},{2,3},{3,2},{4,5},{5,4},{6,7},{7,6},{8,9},{9,8},{10,11... | collective-permute-start | bytes 98312 | tf_op jit(solution)/shard_map/ppermute | solution.py:247
  78.5 2.6 %copy-start.5 = (f32[2048]{0:T(1024)S(1)}, f32[2048]{0:T(1024)}, u32[]{:S(2)}) copy-start(f32[2048]{0:T(1024)} %param.36) | copy-start | bytes 24580
  78.5 2.6 %copy-start.10 = (bf16[1,2048,1024]{2,1,0:T(8,128)(2,1)S(1)}, bf16[1,2048,1024]{2,1,0:T(8,128)(2,1)}, u32[]{:S(2)}) copy-start(bf16[1,2048,1024]{2,1,0:T(8,128)(2,1)} %param.39) | copy-start | bytes 12582916
  78.6 2.0 %collective-permute-start.1 = (bf16[128,2048]{1,0:T(8,128)(2,1)S(1)}, bf16[128,2048]{1,0:T(8,128)(2,1)S(1)}, u32[]{:S(2)}, u32[]{:S(2)}) collective-permute-start(bf16[128,2048]{1,0:T(8,128)(2,1)S(1)} %copy_bitcast_fusion), channel_id=1, source_target_pairs={{0,1},{1,0},{2,3},{3,2},{4,5},{5,4},{6,7},{7,6},{8,9},{9,8},{10,11... | collective-permute-start | bytes 1572872 | tf_op jit(solution)/shard_map/ppermute | solution.py:253
  80.8 3.2 %copy-start.2 = (bf16[128,2048]{1,0:T(8,128)(2,1)}, bf16[128,2048]{1,0:T(8,128)(2,1)S(1)}, u32[]{:S(2)}) copy-start(bf16[128,2048]{1,0:T(8,128)(2,1)S(1)} %get-tuple-element.18) | copy-start | bytes 1572868
  81.1 2.4 %copy-start.11 = (bf16[128,2048]{1,0:T(8,128)(2,1)S(1)}, bf16[128,2048]{1,0:T(8,128)(2,1)}, u32[]{:S(2)}) copy-start(bf16[128,2048]{1,0:T(8,128)(2,1)} %param.42) | copy-start | bytes 1572868
  83.9 7.7 %copy-start.6 = (f32[2048]{0:T(1024)S(1)}, f32[2048]{0:T(1024)}, u32[]{:S(2)}) copy-start(f32[2048]{0:T(1024)} %param.45) | copy-start | bytes 24580
  95.8 2.3 %collective-permute-start.2 = (bf16[256,1024]{1,0:T(8,128)(2,1)}, bf16[256,1024]{1,0:T(8,128)(2,1)}, u32[]{:S(2)}, u32[]{:S(2)}) collective-permute-start(bf16[256,1024]{1,0:T(8,128)(2,1)} %select_convert_fusion), channel_id=1, source_target_pairs={{0,1},{1,0},{2,3},{3,2},{4,5},{5,4},{6,7},{7,6},{8,9},{9,8},{10,11... | collective-permute-start | bytes 1572872 | tf_op jit(solution)/shard_map/ppermute | solution.py:272
  96.6 19.8 %copy-start.3 = (bf16[128,2048]{1,0:T(8,128)(2,1)S(1)}, bf16[128,2048]{1,0:T(8,128)(2,1)}, u32[]{:S(2)}) copy-start(bf16[128,2048]{1,0:T(8,128)(2,1)} %copy-done.2) | copy-start | bytes 1572868

commit v2 on v1

--- a/solution.py
+++ b/solution.py
@@ -80,23 +80,6 @@
     )
 
 
-def exchange_kernel(count, gather, source, landing, send_sem, recv_sem):
-    me = lax.axis_index("ep")
-    meet(count, me)
-
-    def start(step, carry):
-        link(count, me, step, source, landing, send_sem, recv_sem, gather).start()
-        return carry
-
-    def finish(step, carry):
-        link(count, me, step, source, landing, send_sem, recv_sem, gather).wait()
-        return carry
-
-    lax.fori_loop(1, count, start, 0)
-    landing[me] = source[...] if gather else source[me]
-    lax.fori_loop(1, count, finish, 0)
-
-
 def sum_kernel(count, source, total, landing, send_sem, recv_sem):
     me = lax.axis_index("ep")
     meet(count, me)
@@ -121,20 +104,6 @@
 
 def in_vmem():
     return pl.BlockSpec(memory_space=pltpu.VMEM)
-
-
-def exchange(blocks, count, name, gather=False):
-    shape = (count,) + blocks.shape if gather else blocks.shape
-    return pl.pallas_call(
-        functools.partial(exchange_kernel, count, gather),
-        out_shape=jax.ShapeDtypeStruct(shape, blocks.dtype),
-        in_specs=[in_vmem()],
-        out_specs=in_vmem(),
-        scratch_shapes=semaphores(count),
-        compiler_params=pltpu.CompilerParams(
-            collective_id=name, has_side_effects=True, vmem_limit_bytes=16 * 2**20
-        ),
-    )(blocks)
 
 
 def exchange_sum(blocks, count, name):
@@ -148,6 +117,174 @@
             collective_id=name, has_side_effects=True, vmem_limit_bytes=24 * 2**20
         ),
     )(blocks)
+
+
+def project_kernel(
+    count, gates, payload, query, key, value, outgate, thin, landing, total,
+    partial, arriving, send_one, recv_one, send_two, recv_two,
+):
+    me = lax.axis_index("ep")
+    depth = query.shape[0]
+    width = query.shape[1]
+    sequences = payload.shape[1]
+    meet(count, me)
+
+    def start(step, carry):
+        link(count, me, step, payload, landing, send_one, recv_one, False).start()
+        return carry
+
+    def finish(step, carry):
+        link(count, me, step, payload, landing, send_one, recv_one, False).wait()
+        return carry
+
+    lax.fori_loop(1, count, start, 0)
+    landing[me] = payload[me]
+    lax.fori_loop(1, count, finish, 0)
+    rows = landing[:, :, :depth].reshape(count * sequences, depth)
+    small = jnp.dot(rows, thin[...], preferred_element_type=jnp.float32)
+    upper = small.astype(jnp.bfloat16).astype(jnp.float32)
+    place = lax.broadcasted_iota(jnp.int32, small.shape, 1)
+    small = jnp.where(place < gates, upper, small - upper).astype(jnp.bfloat16)
+    partial[:, :, 4 * width :] = small.reshape(count, sequences, small.shape[1])
+    for number, weight in enumerate((query, key, value, outgate)):
+        sums = jnp.dot(rows, weight[...], preferred_element_type=jnp.float32)
+        partial[:, :, number * width : (number + 1) * width] = sums.astype(jnp.bfloat16).reshape(
+            count, sequences, width
+        )
+
+    def start_sum(step, carry):
+        link(count, me, step, partial, arriving, send_two, recv_two, False).start()
+        return carry
+
+    def finish_sum(step, carry):
+        link(count, me, step, partial, arriving, send_two, recv_two, False).wait()
+        total[...] += arriving[lax.rem(me + count - step, count)].astype(jnp.float32)
+        return carry
+
+    lax.fori_loop(1, count, start_sum, 0)
+    total[...] = partial[me].astype(jnp.float32)
+    lax.fori_loop(1, count, finish_sum, 0)
+
+
+def project(payload, weights, thin, count, gates, name):
+    sequences = payload.shape[1]
+    width = 4 * weights[0].shape[1] + thin.shape[1]
+    block = (count, sequences, width)
+    return pl.pallas_call(
+        functools.partial(project_kernel, count, gates),
+        out_shape=(
+            jax.ShapeDtypeStruct(payload.shape, payload.dtype),
+            jax.ShapeDtypeStruct((sequences, width), jnp.float32),
+        ),
+        in_specs=[in_vmem()] * 6,
+        out_specs=(in_vmem(), in_vmem()),
+        scratch_shapes=[pltpu.VMEM(block, jnp.bfloat16)] * 2 + semaphores(count) + semaphores(count),
+        compiler_params=pltpu.CompilerParams(
+            collective_id=name, has_side_effects=True, vmem_limit_bytes=32 * 2**20
+        ),
+    )(payload, *weights, thin)
+
+
+def across(side, source, landing, send_sem, recv_sem):
+    return pltpu.make_async_remote_copy(
+        src_ref=source,
+        dst_ref=landing,
+        send_sem=send_sem,
+        recv_sem=recv_sem,
+        device_id={"tp": 1 - side},
+        device_id_type=pl.DeviceIdType.MESH,
+    )
+
+
+def mix_kernel(
+    count, gated, mix, tokens, gathered, landing, partial, came, mine,
+    send_one, recv_one, send_two, recv_two, send_three, recv_three, send_four, recv_four,
+):
+    me, side = lax.axis_index("ep"), lax.axis_index("tp")
+    barrier = pltpu.get_barrier_semaphore()
+
+    def greet(step, carry):
+        pl.semaphore_signal(
+            barrier,
+            inc=1,
+            device_id={"ep": lax.rem(me + step, count)},
+            device_id_type=pl.DeviceIdType.MESH,
+        )
+        return carry
+
+    lax.fori_loop(1, count, greet, 0)
+    pl.semaphore_signal(
+        barrier, inc=1, device_id={"tp": 1 - side}, device_id_type=pl.DeviceIdType.MESH
+    )
+    pl.semaphore_wait(barrier, count)
+
+    def start(step, carry):
+        link(count, me, step, gated, landing, send_one, recv_one, True).start()
+        return carry
+
+    def finish(step, carry):
+        link(count, me, step, gated, landing, send_one, recv_one, True).wait()
+        return carry
+
+    lax.fori_loop(1, count, start, 0)
+    landing[me] = gated[...]
+    lax.fori_loop(1, count, finish, 0)
+    rows = landing[...].reshape(-1, gated.shape[1])
+    sums = jnp.dot(rows, mix[...], preferred_element_type=jnp.float32)
+    partial[...] = sums.astype(jnp.bfloat16).reshape(partial.shape)
+    swap = across(side, partial.at[1 - side], came, send_two, recv_two)
+    swap.start()
+    swap.wait()
+    attended = partial[side].astype(jnp.float32) + came[...].astype(jnp.float32)
+    residual = (tokens[side].astype(jnp.float32) + attended).astype(jnp.bfloat16)
+    mine[...] = residual
+    own = gathered.at[side]
+
+    def start_rows(step, carry):
+        link(count, me, step, mine, own, send_three, recv_three, True).start()
+        return carry
+
+    def relay(step, carry):
+        link(count, me, step, mine, own, send_three, recv_three, True).wait()
+        origin = lax.rem(me + count - step, count)
+        place = gathered.at[side, origin]
+        across(side, place, place, send_four.at[step], recv_four.at[step]).start()
+        return carry
+
+    def finish_rows(step, carry):
+        place = gathered.at[side, me]
+        across(side, place, place, send_four.at[step], recv_four.at[step]).wait()
+        return carry
+
+    lax.fori_loop(1, count, start_rows, 0)
+    across(side, mine, gathered.at[side, me], send_four.at[0], recv_four.at[0]).start()
+    gathered[side, me] = residual
+    lax.fori_loop(1, count, relay, 0)
+    lax.fori_loop(0, count, finish_rows, 0)
+
+
+def mix_rows(gated, mix, tokens, count, name):
+    half, own_width = tokens.shape[1:]
+    block = pltpu.VMEM((half, own_width), jnp.bfloat16)
+    return pl.pallas_call(
+        functools.partial(mix_kernel, count),
+        out_shape=jax.ShapeDtypeStruct((2, count, half, own_width), jnp.bfloat16),
+        in_specs=[in_vmem()] * 3,
+        out_specs=in_vmem(),
+        scratch_shapes=[
+            pltpu.VMEM((count,) + gated.shape, jnp.bfloat16),
+            pltpu.VMEM((2, half, own_width), jnp.bfloat16),
+            block,
+            block,
+        ]
+        + semaphores(count)
+        + [pltpu.SemaphoreType.DMA, pltpu.SemaphoreType.DMA]
+        + semaphores(count)
+        + semaphores(count),
+        compiler_params=pltpu.CompilerParams(
+            collective_id=name, has_side_effects=True, vmem_limit_bytes=32 * 2**20
+        ),
+    )(gated, mix, tokens)
 
 
 def split_parts(values, number):
@@ -209,27 +346,16 @@
         ],
         axis=2,
     ).transpose(1, 0, 2)
-    columns = exchange(payload, ep_count, 1).reshape(rows, -1)
+    thin = jnp.concatenate((input_weight, forget_weight), axis=1)
+    gates = thin.shape[1]
+    thin = jnp.pad(jnp.concatenate((thin, thin), axis=1), ((0, 0), (0, lanes - 2 * gates)))
+    wide = (query_weight, key_weight, value_weight, outgate_weight)
+    columns, sums = project(payload, wide, thin, ep_count, gates, 1)
+    columns = columns.reshape(rows, -1)
     token_columns = columns[:, own_width : 2 * own_width]
     row_weight = jnp.sum(
         columns[:, 2 * own_width : 2 * own_width + 3].astype(jnp.float32), axis=1, keepdims=True
     )
-
-    wide = jnp.concatenate((query_weight, key_weight, value_weight, outgate_weight), axis=1)
-    thin = jnp.concatenate((input_weight, forget_weight), axis=1)
-    own_columns = columns[:, :own_width]
-    wide_sums = jnp.dot(own_columns, wide, preferred_element_type=jnp.float32)
-    thin_sums = jnp.dot(own_columns, thin, preferred_element_type=jnp.float32)
-    gates = thin.shape[1]
-    upper, under = split_parts(thin_sums, 2)
-    partials = jnp.concatenate(
-        [
-            wide_sums.astype(jnp.bfloat16),
-            jnp.pad(jnp.concatenate([upper, under], axis=1), ((0, 0), (0, lanes - 2 * gates))),
-        ],
-        axis=1,
-    )
-    sums = exchange_sum(partials.reshape(ep_count, sequences, -1), ep_count, 2)
     width = query_weight.shape[1]
     gate_sums = sums[:, 4 * width : 4 * width + gates] + sums[:, 4 * width + gates : 4 * width + 2 * gates]
     projected = tuple(
@@ -237,23 +363,9 @@
     ) + (gate_sums[:, : gates // 2], gate_sums[:, gates // 2 :])
     gated, memory_new, stab_new = memory_step(projected, forget_bias, memory, stabilizer, head_gain)
 
-    all_gated = exchange(gated, ep_count, 3, gather=True).reshape(rows, -1)
-    partial_value = jnp.dot(
-        all_gated, mix_weight, preferred_element_type=jnp.float32
-    ).astype(jnp.bfloat16)
-    half = rows // tp_count
-    upper, under = partial_value[:half], partial_value[half:]
-    kept = jnp.where(first, upper, under)
-    came = lax.ppermute(jnp.where(first, under, upper), "tp", swap)
-    attended = kept.astype(jnp.float32) + came.astype(jnp.float32)
-    token_half = jnp.where(first, token_columns[:half], token_columns[half:])
-    residual_part = (token_half.astype(jnp.float32) + attended).astype(jnp.bfloat16)
-    half_rows = exchange(residual_part, ep_count, 4, gather=True)
-    half_rows = half_rows.transpose(1, 0, 2).reshape(half, model_width)
-    other_rows = lax.ppermute(half_rows, "tp", swap)
-    residual = jnp.concatenate(
-        [jnp.where(first, half_rows, other_rows), jnp.where(first, other_rows, half_rows)], axis=0
-    )
+    token_halves = token_columns.reshape(tp_count, rows // tp_count, own_width)
+    gathered = mix_rows(gated, mix_weight, token_halves, ep_count, 2)
+    residual = gathered.transpose(0, 2, 1, 3).reshape(rows, model_width)
     normed_second = rms_scale(residual.astype(jnp.float32), second_gain).astype(jnp.bfloat16)
 
     gate_pre = jnp.dot(normed_second, expert_gate[0], preferred_element_type=jnp.float32)

time: 119 us -> 121 us (1.017)
  local copies, waits for them, and re-layouts: 1.28 us -> 8.64 us
  waiting for transfers between devices: 4.44 us -> 0.01 us
  Pallas kernels: 80.4 us -> 78.4 us
    pallas_call x2 -> x1, Pallas kernels: 39.9 us -> 17.2 us  [exchange_sum(): pl.pallas_call(functools.partial(sum_kernel, count), out_shape=jax.ShapeD...]
    pallas_call x3 -> x2, Pallas kernels: 40.5 us -> 61.2 us  [the longest x1 31.5 us: mix_rows(): pl.pallas_call(functools.partial(mix_kernel, count), out_shape=jax.ShapeD...]
    unnamed x27 -> x34, local copies, waits for them, and re-layouts: 0.81 us -> 6.88 us
    ppermute x2 -> x0, waiting for transfers between devices: 2.98 us -> none  [the longest x1 1.79 us: body(): other_rows = lax.ppermute(half_rows, 'tp', swap)]
    dot_general x3 -> x0, matrix products: 2.55 us -> none  [the longest x1 1.51 us: body(): wide_sums = jnp.dot(own_columns, wide, preferred_element_type=jnp.float32)]
    dot_general x1, matrix products: 2.34 us -> 4.81 us  [body(): jnp.dot(normed_second, expert_gate[0], preferred_element_type=jnp.float32)]
    ppermute x1, waiting for transfers between devices: 1.46 us -> 0.01 us  [body(): received = lax.ppermute(passed, 'tp', swap).astype(jnp.float32)]
  transfers between devices with their start and end apart: 3 -> 1, of which waited for: 3 -> 0; matrix products, arithmetic and copies ran while one was open for 1% -> 3% of each run, Pallas kernels for 0% -> 0%
where the time goes in v2:
time: 121 us; the launch traced here: 119 us
  Pallas kernels  78.4 us (65%)
  matrix products  19.6 us (16%)
  other arithmetic  10.8 us (9%)
  local copies, waits for them, and re-layouts  8.64 us (7%)
    pallas_call x1, Pallas kernels, mix_rows(): pl.pallas_call(functools.partial(mix_kernel, count), out_shape=jax.ShapeD...  31.5 us
    pallas_call x1, Pallas kernels, project(): pl.pallas_call(functools.partial(project_kernel, count, gates), out_shape...  29.7 us
    pallas_call x1, Pallas kernels, exchange_sum(): pl.pallas_call(functools.partial(sum_kernel, count), out_shape=jax.ShapeD...  17.2 us
    dot_general x1, matrix products, body(): jnp.dot(expert_act, expert_down[0], preferred_element_type=jnp.float32)  7.65 us
    unnamed x34, local copies, waits for them, and re-layouts  6.88 us
    dot_general x1, matrix products, body(): jnp.dot(normed_second, expert_gate[0], preferred_element_type=jnp.float32)  4.81 us
    dot_general x1, matrix products, memory_step(): jnp.einsum('bhvk,bhk->bhv', memory_new, query_heads, precision=lax.Precis...  3.35 us
    dot_general x1, matrix products, body(): jnp.dot(dense_act, dense_down, preferred_element_type=jnp.float32)  3.25 us
  transfers between devices with their start and end apart: 1, of which 0 were waited for; matrix products, arithmetic and copies ran while one was open for 3% of the time, Pallas kernels for 0%

profile of v2, /device:TPU:0, one launch (start us, length us, event | category | flops | bytes accessed | tf_op | source)
XLA Modules:
  0.0 118.8 jit_solution(8665925147326022267)
XLA Ops:
  0.7 1.0 fusion.48
  1.7 0.8 select_reduce_fusion
  2.5 0.8 pad_maximum_fusion.1
  3.6 1.0 copy_bitcast_fusion.1
  4.7 0.9 copy-done.2
  5.6 0.9 copy-done.3
  6.5 0.9 copy-done.4
  7.4 0.9 copy-done.5
  8.3 29.7 %shard_map.238 = (bf16[16,16,384]{2,1,0:T(8,128)(2,1)S(1)}, f32[16,2176]{1,0:T(8,128)S(1)}) custom-call(bf16[16,16,384]{2,1,0:T(8,128)(2,1)S(1)} %fusion.47.payload, bf16[128,512]{1,0:T(8,128)(2,1)S(1)} %copy-done.2, bf16[128,512]{1,0:T(8,128)(2,1)S(1)} %copy-done.3, bf16[128,512]{1,0:T(8,128)(2,1)S(1)} %copy-done.4, bf16[128,512]{1,0:T(8,128)(2,1)S(1)} %copy-done.5, ...), custom_call_target="tpu_custom_call" | custom-call | tf_op jit(solution)/shard_map/pallas_call | solution.py:173
  38.7 3.0 %multiply_add_fusion = f32[16,4,128,128]{3,2,1,0:T(8,128)S(1)} fusion(f32[16,4,128,128]{3,2,1,0:T(8,128)} %param.32, f32[16,4,128]{2,1,0:T(4,128)S(1)} %mul.177, f32[16,4,128]{2,1,0:T(4,128)S(1)} %broadcast_multiply_fusion, f32[16,4]{1,0:T(8,128)S(1)} %get-tuple-element.19), kind=kLoop, calls=%fused_computation.6 | loop fusion | flops 3145728 | bytes 8454400 | tf_op jit(solution)/shard_map/add | solution.py:42
  41.8 3.4 %fusion.70 = f32[16,4,1,128]{3,2,1,0:T(1,128)S(1)} fusion(f32[16,4,128,128]{3,2,1,0:T(8,128)S(1)} %multiply_add_fusion, bf16[16,4,128,1]{2,3,1,0:T(2,128)(2,1)S(1)} %reshape.166), kind=kOutput, calls=%fused_computation.92 | convolution fusion | flops 12582912 | bytes 4243456 | tf_op jit(solution)/shard_map/bhvk,bhk->bhv/dot_general | solution.py:45
  45.4 31.5 %shard_map.239 = bf16[2,16,128,128]{3,2,1,0:T(8,128)(2,1)S(1)} custom-call(bf16[16,512]{1,0:T(8,128)(2,1)S(1)} %bitcast.91, bf16[512,128]{1,0:T(8,128)(2,1)S(1)} %copy-done.1, bf16[2,128,128]{2,1,0:T(8,128)(2,1)S(1)} %bitcast.88), custom_call_target="tpu_custom_call" | custom-call | tf_op jit(solution)/shard_map/pallas_call | solution.py:269
  77.6 0.7 copy.65
  78.3 0.7 copy.64
  79.0 4.8 %fusion.13 = f32[256,1024]{1,0:T(8,128)} fusion(bf16[1,2048,1024]{2,1,0:T(8,128)(2,1)} %param.39, bf16[32,8,16,128]{3,2,1,0:T(8,128)(2,1)S(1)} %bitcast.96), kind=kOutput, calls=%fused_computation.16 | convolution fusion | flops 1074003968 | bytes 6291456 | tf_op jit(solution)/shard_map/dot_general | solution.py:371
  83.8 0.5 fusion.45
  84.4 7.6 %fusion.6 = f32[256,2048]{1,0:T(8,128)} fusion(bf16[1,1024,2048]{2,1,0:T(8,128)(2,1)} %param.41, f32[256]{0:T(256)S(1)} %convert_reduce_fusion, f32[256,1024]{1,0:T(8,128)} %fusion.13, bf16[1,2048,1024]{2,1,0:T(8,128)(2,1)} %param.40, bf16[32,8,16,128]{3,2,1,0:T(8,128)(2,1)S(1)} %bitcast.97), kind=kOutput, calls=%fused_computation.7 | convolution fusion | flops 2150367232 | bytes 12583936 | tf_op jit(solution)/shard_map/dot_general | solution.py:374
  92.0 3.2 %fusion.9 = f32[256,2048]{1,0:T(8,128)S(1)} fusion(f32[256,2048]{1,0:T(8,128)} %fusion.6, bf16[128,2048]{1,0:T(8,128)(2,1)S(1)} %copy-done, bf16[128,2048]{1,0:T(8,128)(2,1)S(1)} %copy-done.8, f32[2048]{0:T(1024)S(1)} %copy-done.10, f32[2048]{0:T(1024)S(1)} %copy-done.9, f32[256]{0:T(256)S(1)} %get-tuple-element.28, f32[256,128]{1,0:T(8,128)S(1)} %fusion.45, ...), kind=kOutput, calls=%fused_computation.9 | convolution fusion | flops 271777792 | bytes 6439936 | tf_op jit(solution)/shard_map/dot_general | solution.py:380
  95.4 0.4 collective-permute-start
  95.8 0.7 copy.66
  96.5 2.5 %copy.95 = bf16[32,8,16,128]{3,1,2,0:T(8,128)(2,1)} copy(bf16[32,8,16,128]{3,2,1,0:T(8,128)(2,1)} %bitcast.94) | data formatting | bytes 2097152
  98.9 1.3 %add_convert_fusion = bf16[256,1024]{1,0:T(8,128)(2,1)S(1)} fusion(bf16[256,1024]{1,0:T(8,128)(2,1)} %collective-permute-done, f32[256,2048]{1,0:T(8,128)S(1)} %fusion.9, pred[]{:T(512)S(6)} %eq.19), kind=kLoop, calls=%fused_computation.27 | loop fusion | flops 1048576 | bytes 3145729 | tf_op jit(solution)/shard_map/convert_element_type | solution.py:385
  100.2 17.2 %shard_map.240 = f32[16,1024]{1,0:T(8,128)S(1)} custom-call(bf16[16,16,1024]{2,1,0:T(8,128)(2,1)S(1)} %bitcast.87), custom_call_target="tpu_custom_call" | custom-call | tf_op jit(solution)/shard_map/pallas_call | solution.py:110
  117.4 1.4 %add_convert_fusion.1 = bf16[16,1024]{1,0:T(8,128)(2,1)} fusion(f32[16,1024]{1,0:T(8,128)S(1)} %shard_map.240, bf16[256,2048]{1,0:T(8,128)(2,1)} %bitcast.95, s32[]{:T(128)S(6)} %select_n.29, s32[]{:T(128)S(6)} %select_n.30), kind=kLoop, calls=%fused_computation.54 | loop fusion | flops 49152 | bytes 131080 | tf_op jit(solution)/shard_map/convert_element_type | solution.py:391
  (56 shorter events, 2.0 us)
Async XLA Ops:
  0.6 91.4 %copy-start = (bf16[128,2048]{1,0:T(8,128)(2,1)S(1)}, bf16[128,2048]{1,0:T(8,128)(2,1)}, u32[]{:S(2)}) copy-start(bf16[128,2048]{1,0:T(8,128)(2,1)} %param.44) | copy-start | bytes 1572868
  0.6 37.7 %copy-start.11 = (f32[16,4]{0,1:T(4,128)S(1)}, f32[16,4]{0,1:T(4,128)}, u32[]{:S(2)}) copy-start(f32[16,4]{0,1:T(4,128)} %param.33) | copy-start | bytes 772
  0.7 37.7 %copy-start.13 = (f32[4]{0:T(128)S(1)}, f32[4]{0:T(128)}, u32[]{:S(2)}) copy-start(f32[4]{0:T(128)} %param.31) | copy-start | bytes 52
  4.7 0.9 copy-start.2
  5.6 0.9 copy-start.3
  6.5 0.9 copy-start.4
  7.4 0.9 copy-start.5
  41.7 3.4 %copy-start.6 = (f32[16,4,128,128]{3,2,1,0:T(8,128)}, f32[16,4,128,128]{3,2,1,0:T(8,128)S(1)}, u32[]{:S(2)}) copy-start(f32[16,4,128,128]{3,2,1,0:T(8,128)S(1)} %multiply_add_fusion) | copy-start | bytes 12582916
  41.8 3.5 %copy-start.12 = (f32[512]{0:T(512)S(1)}, f32[512]{0:T(512)}, u32[]{:S(2)}) copy-start(f32[512]{0:T(512)} %param.34) | copy-start | bytes 6148
  41.8 3.6 %copy-start.1 = (bf16[512,128]{1,0:T(8,128)(2,1)S(1)}, bf16[512,128]{1,0:T(8,128)(2,1)}, u32[]{:S(2)}) copy-start(bf16[512,128]{1,0:T(8,128)(2,1)} %mix.1) | copy-start | bytes 393220
  45.1 32.1 %copy-start.9 = (f32[2048]{0:T(1024)S(1)}, f32[2048]{0:T(1024)}, u32[]{:S(2)}) copy-start(f32[2048]{0:T(1024)} %param.36) | copy-start | bytes 24580
  79.0 4.8 %copy-start.7 = (bf16[2,128,16,128]{3,2,1,0:T(8,128)(2,1)}, bf16[2,128,16,128]{3,2,1,0:T(8,128)(2,1)S(1)}, u32[]{:S(2)}) copy-start(bf16[2,128,16,128]{3,2,1,0:T(8,128)(2,1)S(1)} %copy.64) | copy-start | bytes 3145732
  79.0 4.8 %copy-start.14 = (bf16[128,2048]{1,0:T(8,128)(2,1)S(1)}, bf16[128,2048]{1,0:T(8,128)(2,1)}, u32[]{:S(2)}) copy-start(bf16[128,2048]{1,0:T(8,128)(2,1)} %param.42) | copy-start | bytes 1572868
  84.3 7.7 %copy-start.8 = (bf16[128,2048]{1,0:T(8,128)(2,1)S(1)}, bf16[128,2048]{1,0:T(8,128)(2,1)}, u32[]{:S(2)}) copy-start(bf16[128,2048]{1,0:T(8,128)(2,1)} %param.43) | copy-start | bytes 1572868
  84.4 7.7 %copy-start.10 = (f32[2048]{0:T(1024)S(1)}, f32[2048]{0:T(1024)}, u32[]{:S(2)}) copy-start(f32[2048]{0:T(1024)} %param.45) | copy-start | bytes 24580
  95.4 3.5 %collective-permute-start = (bf16[256,1024]{1,0:T(8,128)(2,1)S(1)}, bf16[256,1024]{1,0:T(8,128)(2,1)}, u32[]{:S(2)}, u32[]{:S(2)}) collective-permute-start(bf16[256,1024]{1,0:T(8,128)(2,1)S(1)} %select_convert_fusion), channel_id=1, source_target_pairs={{0,1},{1,0},{2,3},{3,2},{4,5},{5,4},{6,7},{7,6},{8,9},{9,8},{10,11... | collective-permute-start | bytes 1572872 | tf_op jit(solution)/shard_map/ppermute | solution.py:384
